TPU v7x, 32 devices: a whole 2x2x4 slice. The times are simulated.
32 devices in a mesh: grp: 2 (over x), ep: 8 (over z, y), tp: 2 (over core).
Axes of the slice: x: 2, y: 2, z: 4, core: 2. Of those that a mesh axis runs over, the one named last changes fastest.
Arguments:
- tokens: bfloat16 [4096, 2048], P(('grp', 'ep', 'tp')), parts along dimension 0, may hold values from -6 to 6
- expert_ids: int32 [4096, 4], P(('grp', 'ep', 'tp')), parts along dimension 0, may hold values from 0 to 15, all different within a row; in each aligned block of 128 rows (0 to 127, 128 to 255, ...) at most 64 rows name the same one
- route_weights: float32 [4096, 4], P(('grp', 'ep', 'tp')), parts along dimension 0, may hold values from 0.05 to 1
- norm_gain: float32 [2048], replicated, may hold values from 0.1 to 1.9
- w_gate: bfloat16 [16, 2048, 896], P(('ep', 'tp')), may hold values from -0.5 to 0.5
- w_up: bfloat16 [16, 2048, 896], P(('ep', 'tp')), may hold values from -0.5 to 0.5
- w_down: bfloat16 [16, 896, 2048], P(('ep', 'tp')), may hold values from -0.0234375 to 0.0234375
Outputs:
- mixed: bfloat16 [4096, 2048], P(('grp', 'ep', 'tp')), parts along dimension 0
There are 2 independent parts, one for each index of `grp`. A program takes and returns all parts, laid end to end along the dimension named above; an argument that names none is the same for every part. Nothing has to cross between parts.
Inputs may be any that keep to these rules, and one draw needn't show every extreme that they name: `expert_ids`: each token names 4 different experts. Among the 128 tokens of one device (aligned blocks of rows) no expert is named more than 64 times, a bound that some block reaches.
All inputs are finite; a program needn't handle non-finite values.
Results may differ from a plain program's by a relative error of at most 0.0071.
Values may be sent and summed in bfloat16 or wider, within the bound.
A program may use at most 64 MiB of HBM per device.

v0:
```python
import jax
import jax.numpy as jnp
from jax import lax
from jax.sharding import PartitionSpec as P

norm_eps = 1e-05
clamp_limit = 7.0
sig_alpha = 1.702


def layer_norm(tokens, norm_gain):
    values = tokens.astype(jnp.float32)
    row_mean = jnp.mean(values, -1, keepdims=True)
    centred = values - row_mean
    row_var = jnp.mean(centred * centred, -1, keepdims=True)
    scaled = centred * lax.rsqrt(row_var + norm_eps) * norm_gain
    return scaled.astype(jnp.bfloat16)


def expert_apply(inputs, gate_mat, up_mat, down_mat):
    gate_pre = jnp.dot(inputs, gate_mat, preferred_element_type=jnp.float32)
    up_pre = jnp.dot(inputs, up_mat, preferred_element_type=jnp.float32)
    gated = jnp.minimum(gate_pre, clamp_limit)
    upper = jnp.clip(up_pre, -clamp_limit, clamp_limit)
    hidden = (gated * jax.nn.sigmoid(sig_alpha * gated) * (upper + 1.0)).astype(jnp.bfloat16)
    return jnp.dot(hidden, down_mat, preferred_element_type=jnp.float32).astype(jnp.bfloat16)


def local(tokens, expert_ids, route_weights, norm_gain, w_gate, w_up, w_down):
    ep_count = lax.axis_size("ep")
    tp_count = lax.axis_size("tp")
    experts = ep_count * tp_count
    tok_rows, feat_width = tokens.shape
    top_count = expert_ids.shape[1]
    capacity = 2 * tok_rows * top_count // experts
    normed = layer_norm(tokens, norm_gain)
    flat_ids = expert_ids.reshape(-1)
    one_hot = (flat_ids[:, None] == jnp.arange(experts, dtype=jnp.int32)[None, :]).astype(jnp.int32)
    slot_index = jnp.sum((jnp.cumsum(one_hot, 0) - one_hot) * one_hot, 1)
    target = flat_ids * capacity + slot_index
    pair_token = jnp.arange(tok_rows * top_count, dtype=jnp.int32) // top_count
    buffer = (
        jnp.zeros((experts * capacity, feat_width), jnp.bfloat16).at[target].set(normed[pair_token])
    )
    buffer = buffer.reshape(experts, capacity, feat_width)
    gate_mat = w_gate[0]
    up_mat = w_up[0]
    down_mat = w_down[0]
    arrived = lax.all_to_all(buffer, ("ep", "tp"), split_axis=0, concat_axis=0, tiled=True)
    flat_rows = arrived.reshape(-1, feat_width)
    returned = lax.all_to_all(
        expert_apply(flat_rows, gate_mat, up_mat, down_mat).reshape(arrived.shape),
        ("ep", "tp"),
        split_axis=0,
        concat_axis=0,
        tiled=True,
    )
    picked = returned.reshape(experts * capacity, feat_width)[target].reshape(
        tok_rows, top_count, feat_width
    )
    combined = jnp.zeros((tok_rows, feat_width), jnp.float32)
    for choice_slot in range(top_count):
        combined = combined + route_weights[:, choice_slot : choice_slot + 1] * picked[
            :, choice_slot
        ].astype(jnp.float32)
    return combined.astype(jnp.bfloat16)


def solution(mesh):
    placed = (
        P(("grp", "ep", "tp"), None),
        P(("grp", "ep", "tp"), None),
        P(("grp", "ep", "tp"), None),
        P(),
        P(("ep", "tp"), None, None),
        P(("ep", "tp"), None, None),
        P(("ep", "tp"), None, None),
    )
    return jax.shard_map(
        local, mesh=mesh, in_specs=placed, out_specs=P(("grp", "ep", "tp"), None), check_vma=False
    )
```

profile of v0, /device:TPU:15, one launch (start us, length us, event | category | flops | bytes accessed | tf_op | source)
XLA Modules:
  0.0 249.6 jit_solution(3298156743053346114)
XLA Ops:
  0.0 0.8 copy.13
  0.8 0.1 eq.29
  0.9 0.1 eq.25
  1.0 0.7 broadcast_multiply_fusion
  1.7 1.2 reduce-window.6
  2.9 0.2 slice_reduce_fusion
  3.1 0.1 copy.12
  3.2 0.1 mul.94
  3.4 1.2 convert_reduce_fusion
  4.6 1.3 fusion.12
  5.9 0.1 fusion.21
  6.0 1.4 fusion.14
  7.4 12.8 %scatter_custom_fusion = bf16[1024,2048]{1,0:T(8,128)(2,1)} fusion(s32[512]{0:T(512)S(1)} %bitcast.72, bf16[128,2048]{1,0:T(8,128)(2,1)S(1)} %fusion.14, s32[1024]{0:T(1024)S(1)} %pad_clamp_fusion.1, bf16[]{:T(256)} %constant.15.clone.1), kind=kCustom, calls=%fused_computation.10 | custom fusion | bytes 4194306 | tf_op jit(solution)/shard_map/scatter | solution.py:43
  20.2 0.0 copy-start.1
  20.2 99.0 %all_to_all.10 = bf16[16,64,2048]{2,1,0:T(8,128)(2,1)S(1)} all-to-all(bf16[16,64,2048]{2,1,0:T(8,128)(2,1)} %bitcast.68), channel_id=1, replica_groups=mesh['grp'=2,'ep'=8,'tp'=2] {'ep','tp'}, dimensions={0} | all-to-all | bytes 8388608 | tf_op jit(solution)/shard_map/all_to_all | solution.py:49
  119.2 0.0 copy-done.1
  119.2 0.0 copy-start.2
  119.2 4.5 %fusion.1 = f32[1024,896]{1,0:T(8,128)S(1)} fusion(bf16[1024,2048]{1,0:T(8,128)(2,1)S(1)} %bitcast.70, bf16[1,2048,896]{2,1,0:T(8,128)(2,1)S(1)} %copy-done.1), kind=kOutput, calls=%fused_computation.5 | convolution fusion | flops 3758096384 | bytes 11534336 | tf_op jit(solution)/shard_map/dot_general | solution.py:22
  123.7 0.0 copy-done.2
  123.7 0.0 copy-start.3
  123.8 5.1 %multiply_convert_fusion = bf16[1024,896]{1,0:T(8,128)(2,1)S(1)} fusion(f32[1024,896]{1,0:T(8,128)S(1)} %fusion.1, bf16[1024,2048]{1,0:T(8,128)(2,1)S(1)} %bitcast.71, bf16[1,2048,896]{2,1,0:T(8,128)(2,1)S(1)} %copy-done.2), kind=kOutput, calls=%fused_computation.9 | convolution fusion | flops 3767271424 | bytes 13369344 | tf_op jit(solution)/shard_map/dot_general | solution.py:21
  128.9 0.0 copy-done.3
  128.9 6.1 %convolution_convert_fusion = bf16[1024,2048]{1,0:T(8,128)(2,1)} fusion(bf16[1024,896]{1,0:T(8,128)(2,1)S(1)} %multiply_convert_fusion, bf16[1,896,2048]{2,1,0:T(8,128)(2,1)S(1)} %copy-done.3), kind=kOutput, calls=%fused_computation.3 | convolution fusion | flops 3760193536 | bytes 9699328 | tf_op jit(solution)/shard_map/dot_general | solution.py:26
  135.0 0.0 copy-start
  135.0 5.3 %all-to-all-start.1 = ((bf16[16,64,2048]{2,1,0:T(8,128)(2,1)}), bf16[16,64,2048]{2,1,0:T(8,128)(2,1)}, u32[]{:S(2)}, u32[]{:S(2)}) async-start(bf16[16,64,2048]{2,1,0:T(8,128)(2,1)} %bitcast.69), calls=%async_computation.1 | async-start | bytes 8388608 | tf_op jit(solution)/shard_map/all_to_all | solution.py:51
  140.3 0.0 copy-done
  140.4 92.4 %all-to-all-done.1 = bf16[16,64,2048]{2,1,0:T(8,128)(2,1)} async-done(((bf16[16,64,2048]{2,1,0:T(8,128)(2,1)}), bf16[16,64,2048]{2,1,0:T(8,128)(2,1)}, u32[]{:S(2)}, u32[]{:S(2)}) %all-to-all-start.1) | async-done | bytes 4194336 | tf_op jit(solution)/shard_map/all_to_all | solution.py:51
  232.8 8.0 %gather_fusion = bf16[512,2048]{1,0:T(8,128)(2,1)} fusion(bf16[1024,2048]{1,0:T(8,128)(2,1)} %bitcast.11, s32[1024]{0:T(1024)S(1)} %pad_clamp_fusion), kind=kCustom, calls=%fused_computation.1 | custom fusion | bytes 4196352 | tf_op jit(solution)/shard_map/gather | solution.py:58
  240.8 2.7 %reshape.130 = bf16[128,4,2048]{2,1,0:T(4,128)(2,1)S(1)} reshape(bf16[512,2048]{1,0:T(8,128)(2,1)} %gather_fusion) | data formatting | bytes 4194304 | tf_op jit(solution)/shard_map/reshape | solution.py:58
  243.5 3.1 %fusion.23 = (bf16[128,1,2048]{2,1,0:T(2,128)(2,1)S(1)}, bf16[128,1,2048]{2,1,0:T(2,128)(2,1)S(1)}, bf16[128,1,2048]{2,1,0:T(2,128)(2,1)S(1)}, bf16[128,1,2048]{2,1,0:T(2,128)(2,1)S(1)}) fusion(bf16[128,4,2048]{2,1,0:T(4,128)(2,1)S(1)} %reshape.130), kind=kLoop, calls=%fused_computation.56 | loop fusion | bytes 4194304 | tf_op jit(solution)/shard_map/slice | solution.py:63
  246.6 3.0 %fusion.16 = bf16[128,2048]{1,0:T(8,128)(2,1)} fusion(bf16[128,1,2048]{2,1,0:T(2,128)(2,1)S(1)} %get-tuple-element.8, bf16[128,1,2048]{2,1,0:T(2,128)(2,1)S(1)} %get-tuple-element.6, bf16[128,1,2048]{2,1,0:T(2,128)(2,1)S(1)} %get-tuple-element.7, bf16[128,1,2048]{2,1,0:T(2,128)(2,1)S(1)} %get-tuple-element.5, f32[128]{0:T(128)S(1)} %get-tuple-element.11, ...), kind=kLoop, calls=%fused_computation.22 | loop fusion | flops 3145728 | bytes 2623488 | tf_op jit(solution)/shard_map/convert_element_type | solution.py:66
  (10 shorter events, 0.1 us)
Async XLA Ops:
  20.2 99.0 %copy-start.1 = (bf16[1,2048,896]{2,1,0:T(8,128)(2,1)S(1)}, bf16[1,2048,896]{2,1,0:T(8,128)(2,1)}, u32[]{:S(2)}) copy-start(bf16[1,2048,896]{2,1,0:T(8,128)(2,1)} %param.12) | copy-start | bytes 11010052
  119.2 4.5 %copy-start.2 = (bf16[1,2048,896]{2,1,0:T(8,128)(2,1)S(1)}, bf16[1,2048,896]{2,1,0:T(8,128)(2,1)}, u32[]{:S(2)}) copy-start(bf16[1,2048,896]{2,1,0:T(8,128)(2,1)} %param.11) | copy-start | bytes 11010052
  123.7 5.2 %copy-start.3 = (bf16[1,896,2048]{2,1,0:T(8,128)(2,1)S(1)}, bf16[1,896,2048]{2,1,0:T(8,128)(2,1)}, u32[]{:S(2)}) copy-start(bf16[1,896,2048]{2,1,0:T(8,128)(2,1)} %param.13) | copy-start | bytes 11010052
  135.0 5.4 %copy-start = (f32[128,4]{0,1:T(4,128)S(1)}, f32[128,4]{0,1:T(4,128)}, u32[]{:S(2)}) copy-start(f32[128,4]{0,1:T(4,128)} %param.9) | copy-start | bytes 6148
  135.0 97.8 %all-to-all-start.1 = ((bf16[16,64,2048]{2,1,0:T(8,128)(2,1)}), bf16[16,64,2048]{2,1,0:T(8,128)(2,1)}, u32[]{:S(2)}, u32[]{:S(2)}) async-start(bf16[16,64,2048]{2,1,0:T(8,128)(2,1)} %bitcast.69), calls=%async_computation.1 | async-start | bytes 8388608 | tf_op jit(solution)/shard_map/all_to_all | solution.py:51
where the time goes:
time: 250 us
  blocking collectives  99 us (40%)
  waiting for transfers between devices  92.4 us (37%)
  local copies, waits for them, and re-layouts  28.1 us (11%)
  matrix products  15.7 us (6%)
  other arithmetic  8.94 us (4%)
  starting transfers between devices  5.35 us (2%)
    all_to_all x1, blocking collectives, local(): lax.all_to_all(buffer, ('ep', 'tp'), split_axis=0, concat_axis=0, tiled=T...  99 us
    all_to_all x1, waiting for transfers between devices, local(): lax.all_to_all(expert_apply(flat_rows, gate_mat, up_mat, down_mat).reshap...  92.4 us
    scatter x1, local copies, waits for them, and re-layouts, local(): jnp.zeros((experts * capacity, feat_width), jnp.bfloat16).at[target]  12.8 us
    gather x1, local copies, waits for them, and re-layouts, local(): returned.reshape(experts * capacity, feat_width)[target]  8 us
    dot_general x1, matrix products, expert_apply(): jnp.dot(hidden, down_mat, preferred_element_type=jnp.float32)  6.07 us
    all_to_all x1, starting transfers between devices, local(): lax.all_to_all(expert_apply(flat_rows, gate_mat, up_mat, down_mat).reshap...  5.35 us
    dot_general x1, matrix products, expert_apply(): gate_pre = jnp.dot(inputs, gate_mat, preferred_element_type=jnp.float32)  5.14 us
  transfers between devices with their start and end apart: 1, of which 1 were waited for; matrix products, arithmetic and copies ran while one was open for 0% of the time, Pallas kernels for 0%

commit v1 on v0

--- a/solution.py
+++ b/solution.py
@@ -26,7 +26,7 @@
     return jnp.dot(hidden, down_mat, preferred_element_type=jnp.float32).astype(jnp.bfloat16)
 
 
-def local(tokens, expert_ids, route_weights, norm_gain, w_gate, w_up, w_down):
+def local_exchange(tokens, expert_ids, route_weights, norm_gain, w_gate, w_up, w_down):
     ep_count = lax.axis_size("ep")
     tp_count = lax.axis_size("tp")
     experts = ep_count * tp_count
@@ -66,6 +66,27 @@
     return combined.astype(jnp.bfloat16)
 
 
+def local_gather(tokens, expert_ids, route_weights, norm_gain, w_gate, w_up, w_down):
+    axes = ("ep", "tp")
+    experts = lax.axis_size("ep") * lax.axis_size("tp")
+    normed = layer_norm(tokens, norm_gain)
+    chosen = expert_ids[:, :, None] == jnp.arange(experts, dtype=jnp.int32)
+    dense = jnp.sum(jnp.where(chosen, route_weights[:, :, None], 0.0), 1)
+    factor = lax.all_to_all(dense, axes, split_axis=1, concat_axis=0, tiled=True)
+    gathered = lax.all_gather(normed, axes, axis=0, tiled=True)
+    results = expert_apply(gathered, w_gate[0], w_up[0], w_down[0])
+    scaled = (factor * results.astype(jnp.float32)).astype(jnp.bfloat16)
+    return lax.psum_scatter(scaled, axes, scatter_dimension=0, tiled=True)
+
+
+def local(tokens, expert_ids, *rest):
+    experts = lax.axis_size("ep") * lax.axis_size("tp")
+    tok_rows, top_count = expert_ids.shape
+    capacity = 2 * tok_rows * top_count // experts
+    whole_blocks = lax.axis_size("tp") * capacity >= tok_rows
+    return (local_gather if whole_blocks else local_exchange)(tokens, expert_ids, *rest)
+
+
 def solution(mesh):
     placed = (
         P(("grp", "ep", "tp"), None),

time: 250 us -> 238 us (0.952)
  blocking collectives: 99 us -> 0 us
  waiting for transfers between devices: 92.4 us -> 170 us
  local copies, waits for them, and re-layouts: 28.1 us -> 0 us
  matrix products: 15.7 us -> 40 us
  between operations: 0.12 us -> 13.4 us
  other arithmetic: 8.94 us -> 6.05 us
    reduce_scatter x0 -> x1, waiting for transfers between devices: none -> 103 us  [local_gather(): return lax.psum_scatter(scaled, axes, scatter_dimension=0, tiled=True)]
    all_to_all x1 -> x0, blocking collectives: 99 us -> none  [local(): lax.all_to_all(buffer, ('ep', 'tp'), split_axis=0, concat_axis=0, tiled=T...]
    all_to_all x1, waiting for transfers between devices: 92.4 us -> 0.01 us  [local_gather(): lax.all_to_all(dense, axes, split_axis=1, concat_axis=0, tiled=True)]
    all_gather x0 -> x1, waiting for transfers between devices: none -> 66.9 us  [local_gather(): gathered = lax.all_gather(normed, axes, axis=0, tiled=True)]
    dot_general x1, matrix products: 6.07 us -> 25.9 us  [expert_apply(): jnp.dot(hidden, down_mat, preferred_element_type=jnp.float32)]
    scatter x1 -> x0, local copies, waits for them, and re-layouts: 12.8 us -> none  [local(): jnp.zeros((experts * capacity, feat_width), jnp.bfloat16).at[target]]
    dot_general x1, matrix products: 5.14 us -> 14.1 us  [expert_apply(): gate_pre = jnp.dot(inputs, gate_mat, preferred_element_type=jnp.float32)]
    gather x1 -> x0, local copies, waits for them, and re-layouts: 8 us -> none  [local(): returned.reshape(experts * capacity, feat_width)[target]]
  transfers between devices with their start and end apart: 1 -> 3, of which waited for: 1 -> 2; matrix products, arithmetic and copies ran while one was open for 0% -> 7% of each run, Pallas kernels for 0% -> 0%
where the time goes in v1:
time: 238 us; the launch traced here: 236 us
  waiting for transfers between devices  170 us (71%)
  matrix products  40 us (17%)
  between operations  13.4 us (6%)
  starting transfers between devices  6.56 us (3%)
  other arithmetic  6.05 us (3%)
    reduce_scatter x1, waiting for transfers between devices, local_gather(): return lax.psum_scatter(scaled, axes, scatter_dimension=0, tiled=True)  103 us
    all_gather x1, waiting for transfers between devices, local_gather(): gathered = lax.all_gather(normed, axes, axis=0, tiled=True)  66.9 us
    dot_general x1, matrix products, expert_apply(): jnp.dot(hidden, down_mat, preferred_element_type=jnp.float32)  25.9 us
    dot_general x1, matrix products, expert_apply(): gate_pre = jnp.dot(inputs, gate_mat, preferred_element_type=jnp.float32)  14.1 us
    all_to_all x1, starting transfers between devices, local_gather(): lax.all_to_all(dense, axes, split_axis=1, concat_axis=0, tiled=True)  6.52 us
  transfers between devices with their start and end apart: 3, of which 2 were waited for; matrix products, arithmetic and copies ran while one was open for 7% of the time, Pallas kernels for 0%

profile of v1, /device:TPU:15, one launch (start us, length us, event | category | flops | bytes accessed | tf_op | source)
XLA Modules:
  0.0 235.8 jit_solution(3048979541627226221)
XLA Ops:
  6.5 0.0 all-gather.2.cloned.1.call-start
  6.5 1.2 convert_reduce_fusion
  7.7 1.3 fusion.11
  9.1 2.2 fusion.13
  11.3 0.0 all-gather.2.cloned.1.call-update
  11.3 1.3 select_reduce_fusion
  12.6 6.5 %all-to-all-start = ((f32[128,16,1]{0,2,1:T(1,128)}), f32[128,16,1]{0,2,1:T(1,128)S(1)}, u32[]{:S(2)}, u32[]{:S(2)}) async-start(f32[128,16,1]{0,2,1:T(1,128)} %bitcast.1), calls=%async_computation | async-start | bytes 16384 | tf_op jit(solution)/shard_map/all_to_all | solution.py:75
  19.1 0.0 reduce-scatter.2.cloned.1.call-start
  19.2 66.9 %all-gather.2.cloned.1.call-done = bf16[2048,2048]{1,0:T(8,128)(2,1)} async-done(((bf16[128,2048]{1,0:T(8,128)(2,1)}), bf16[2048,2048]{1,0:T(8,128)(2,1)}) %all-gather.2.cloned.1.call-update) | async-done | bytes 8388624 | tf_op jit(solution)/shard_map/all_gather | solution.py:76
  86.1 14.1 %fusion.3 = f32[2048,896]{1,0:T(8,128)} fusion(bf16[2048,2048]{1,0:T(8,128)(2,1)} %all-gather.2.cloned.1.call-done, bf16[1,2048,896]{2,1,0:T(8,128)(2,1)} %param.11), kind=kOutput, calls=%fused_computation.4 | convolution fusion | flops 7516192768 | bytes 19398656 | tf_op jit(solution)/shard_map/dot_general | solution.py:21
  100.2 0.0 all-to-all-done
  100.2 25.9 %multiply_convert_fusion = bf16[2048,2048]{1,0:T(8,128)(2,1)} fusion(f32[2048]{0:T(1024)S(1)} %bitcast.20, f32[2048,896]{1,0:T(8,128)} %fusion.3, bf16[2048,2048]{1,0:T(8,128)(2,1)} %all-gather.2.cloned.1.call-done, bf16[1,896,2048]{2,1,0:T(8,128)(2,1)} %param.13, bf16[1,2048,896]{2,1,0:T(8,128)(2,1)} %param.12), kind=kOutput, calls=%fused_computation | convolution fusion | flops 15067512832 | bytes 31465472 | tf_op jit(solution)/shard_map/dot_general | solution.py:26
  126.1 0.0 reduce-scatter.2.cloned.1.call-update
  126.2 102.8 %reduce-scatter.2.cloned.1.call-done = bf16[128,2048]{1,0:T(8,128)(2,1)} async-done(((bf16[2048,2048]{1,0:T(8,128)(2,1)}), bf16[128,2048]{1,0:T(8,128)(2,1)}) %reduce-scatter.2.cloned.1.call-update) | async-done | bytes 524304 | tf_op jit(solution)/shard_map/reduce_scatter | solution.py:79
  (2 shorter events, 0.0 us)
Async XLA Ops:
  6.5 79.6 %all-gather.2.cloned.1.call-start = ((), (), s32[]{:S(2)}) async-start(), calls=%async_computation.2 | async-start | bytes 8912896 | tf_op jit(solution)/shard_map/all_gather | solution.py:76
  12.6 87.6 %all-to-all-start = ((f32[128,16,1]{0,2,1:T(1,128)}), f32[128,16,1]{0,2,1:T(1,128)S(1)}, u32[]{:S(2)}, u32[]{:S(2)}) async-start(f32[128,16,1]{0,2,1:T(1,128)} %bitcast.1), calls=%async_computation | async-start | bytes 16384 | tf_op jit(solution)/shard_map/all_to_all | solution.py:75
  19.1 209.8 %reduce-scatter.2.cloned.1.call-start = ((), (), s32[]{:S(2)}) async-start(), calls=%async_computation.3 | async-start | bytes 8912896 | tf_op jit(solution)/shard_map/reduce_scatter | solution.py:79
Sparse Core Ops, SparseCore 0:
  11.4 74.6 all-gather.1
  126.3 102.5 reduce-scatter.1
